TPU v7x, 256 devices: a whole 4x4x8 slice. The times are simulated.
256 devices in a mesh: sp: 32 (over z, x), tp: 8 (over y, core).
Axes of the slice: x: 4, y: 4, z: 8, core: 2. Of those that a mesh axis runs over, the one named last changes fastest.
Arguments:
- latents: bfloat16 [16384, 2048], P(('sp', 'tp')), may hold values from -6 to 6
- context: bfloat16 [512, 2048], P('sp'), may hold values from -6 to 6
- cond: float32 [2048], P('sp'), may hold values from -6 to 6
- ctx_cond: float32 [2048], P('sp'), may hold values from -6 to 6
- mod_weight: float32 [2048, 6144], P('sp', 'tp'), may hold values from -0.125 to 0.125
- query_weight: bfloat16 [2048, 2048], P(None, 'tp'), may hold values from -1 to 1, as said below
- key_matrix: bfloat16 [2048, 1024], P(None, 'tp'), may hold values from -1 to 1, as said below
- value_matrix: bfloat16 [2048, 1024], P(None, 'tp'), may hold values from -0.125 to 0.125
- out_weight: bfloat16 [2048, 2048], P('tp'), may hold values from -0.125 to 0.125
- query_gain: float32 [128], replicated, may hold values from 0.7 to 7
- key_gain: float32 [128], replicated, may hold values from 0.7 to 7
Outputs:
- updated: bfloat16 [16384, 2048], P(('sp', 'tp'))
Inputs may be any that keep to these rules, and one draw needn't show every extreme that they name: `query_weight`: entries of order 2048 to the power -1/2. `key_matrix`: entries of order 2048 to the power -1/2.
All inputs are finite; a program needn't handle non-finite values.
Results may differ from a plain program's by a relative error of at most 0.0085.
The roundings to bfloat16 on the way count: a program that leaves them out, or rounds other values in their place, can miss the bound.
Values may be sent and summed in bfloat16 or wider, within the bound.
No kernel may reach another device: no remote copies, remote signals or barrier semaphores. Data moves between devices by JAX's collectives and lax.ppermute only.
A program may use at most 128 MiB of HBM per device.

v0:
```python
import math
import jax
import jax.numpy as jnp
from jax import lax
from jax.sharding import Mesh
from jax.sharding import PartitionSpec as P

GRID_W = 64
SP = ("sp_0", "sp_1")
SP_TP = ("sp_0", "sp_1", "tp")
NORM_EPS = 1e-06
ROPE_BASE = 10000.0


def over_axes(value, axes):
    for axis in axes:
        value = lax.psum(value, axis)
    return value


def side_by_side(arrays, axis, dim, along):
    both = jnp.concatenate(arrays, axis=along)
    filled, at, done = (lax.all_gather(both, axis, axis=dim, tiled=True), 0, [])
    for a in arrays:
        done.append(lax.slice_in_dim(filled, at, at + a.shape[along], axis=along))
        at += a.shape[along]
    return tuple(done)


def normalize(latent_value_rows):
    return latent_value_rows * lax.rsqrt(
        jnp.mean(latent_value_rows * latent_value_rows, axis=-1, keepdims=True) + NORM_EPS
    )


def rotate(latent_value_rows, positions):
    quarter = latent_value_rows.shape[-1] // 2
    inv_freq = ROPE_BASE ** (-jnp.arange(quarter, dtype=jnp.float32) / quarter)
    angles = positions.astype(jnp.float32)[:, None] * inv_freq[None, :]
    cos_table = jnp.cos(angles)[:, None, :]
    sin_table = jnp.sin(angles)[:, None, :]
    first, second = (latent_value_rows[..., :quarter], latent_value_rows[..., quarter:])
    return jnp.concatenate(
        [first * cos_table - second * sin_table, second * cos_table + first * sin_table], axis=-1
    )


def axial(latent_value_rows, positions):
    half_dim = latent_value_rows.shape[-1] // 2
    return jnp.concatenate(
        [
            rotate(latent_value_rows[..., :half_dim], positions // GRID_W),
            rotate(latent_value_rows[..., half_dim:], positions % GRID_W),
        ],
        axis=-1,
    )


def modulate(latent_value_rows, mod_row):
    model_width = latent_value_rows.shape[-1]
    shift_vec = mod_row[:model_width]
    scale_vec = mod_row[model_width : 2 * model_width]
    return (
        normalize(latent_value_rows.astype(jnp.float32)) * (1.0 + scale_vec) + shift_vec
    ).astype(jnp.bfloat16)


def body(
    latents,
    context,
    cond,
    ctx_cond,
    mod_weight,
    query_weight,
    key_matrix,
    value_matrix,
    out_weight,
    query_gain,
    key_gain,
):
    model_width = latents.shape[1]
    head_dim = query_gain.shape[0]
    sp_count = lax.axis_size(SP)
    partials = jnp.dot(
        jax.nn.silu(jnp.stack([cond, ctx_cond])), mod_weight, precision=lax.Precision.HIGHEST
    )
    summed = over_axes(partials, SP)
    modulation = lax.all_gather(summed, "tp", axis=1, tiled=True)
    gate_vec = modulation[0, 2 * model_width :]
    normalised_rows = modulate(latents, modulation[0])
    prefix_normalised = modulate(context, modulation[1])
    query_cols = query_weight.shape[1]
    key_cols = key_matrix.shape[1]
    piece = lax.all_gather(normalised_rows, "tp", axis=0, tiled=True)
    projected = jnp.concatenate(
        [
            jnp.dot(piece, query_weight, preferred_element_type=jnp.float32),
            jnp.dot(piece, key_matrix, preferred_element_type=jnp.float32),
            jnp.dot(piece, value_matrix, preferred_element_type=jnp.float32),
        ],
        axis=1,
    )
    row_count = projected.shape[0]
    positions = lax.axis_index(SP) * row_count + jnp.arange(row_count, dtype=jnp.int32)
    query_heads = projected[:, :query_cols].reshape(row_count, -1, head_dim)
    query_heads = axial(normalize(query_heads) * query_gain, positions).astype(jnp.bfloat16)
    key_heads = projected[:, query_cols : query_cols + key_cols].reshape(row_count, -1, head_dim)
    key_heads = axial(normalize(key_heads) * key_gain, positions).astype(jnp.bfloat16)
    value_heads = (
        projected[:, query_cols + key_cols :].reshape(row_count, -1, head_dim).astype(jnp.bfloat16)
    )
    key_part = jnp.dot(prefix_normalised, key_matrix, preferred_element_type=jnp.float32).reshape(
        prefix_normalised.shape[0], -1, head_dim
    )
    value_part = jnp.dot(
        prefix_normalised, value_matrix, preferred_element_type=jnp.float32
    ).reshape(prefix_normalised.shape[0], -1, head_dim)
    local_keys = (normalize(key_part) * key_gain).astype(jnp.bfloat16)
    local_values = value_part.astype(jnp.bfloat16)
    prefix_keys, prefix_values = side_by_side((local_keys, local_values), SP, 0, 1)
    kv_local = key_heads.shape[1]
    group_size = query_heads.shape[1] // kv_local
    grouped = query_heads.reshape(row_count, kv_local, group_size, head_dim).transpose(1, 2, 0, 3)
    grouped = grouped.reshape(kv_local, group_size * row_count, head_dim)
    inv_root = head_dim ** (-0.5)
    lift = math.log(sp_count * row_count / (2.0 * prefix_keys.shape[0]))
    ctx_scores = (
        jnp.einsum("hqd,khd->hqk", grouped, prefix_keys, preferred_element_type=jnp.float32)
        * inv_root
        + lift
    )
    top_init = jnp.max(ctx_scores, axis=-1)
    ctx_weights = jnp.exp(ctx_scores - top_init[..., None])
    initial = (
        top_init,
        jnp.sum(ctx_weights, axis=-1),
        jnp.einsum(
            "hqk,khd->hqd",
            ctx_weights.astype(jnp.bfloat16),
            prefix_values,
            preferred_element_type=jnp.float32,
        ),
    )

    def update(state_now, key_block, value_block):
        top_old, total_old, acc_old = state_now
        scores = (
            jnp.einsum("hqd,khd->hqk", grouped, key_block, preferred_element_type=jnp.float32)
            * inv_root
        )
        top_new = jnp.maximum(top_old, jnp.max(scores, axis=-1))
        factor = jnp.exp(top_old - top_new)
        weights_now = jnp.exp(scores - top_new[..., None])
        acc_new = acc_old * factor[..., None] + jnp.einsum(
            "hqk,khd->hqd",
            weights_now.astype(jnp.bfloat16),
            value_block,
            preferred_element_type=jnp.float32,
        )
        return (top_new, total_old * factor + jnp.sum(weights_now, axis=-1), acc_new)

    key_piece, value_piece = side_by_side((key_heads, value_heads), SP, 0, 1)
    key_count = key_piece.shape[0]
    rows_per_block = math.gcd(key_count, 2048)
    block_count = key_count // rows_per_block
    key_blocks = key_piece.reshape(block_count, rows_per_block, kv_local, head_dim)
    value_blocks = value_piece.reshape(block_count, rows_per_block, kv_local, head_dim)

    def one_step(state_in, blocks_in):
        return (update(state_in, blocks_in[0], blocks_in[1]), None)

    state_out, _ = lax.scan(one_step, initial, (key_blocks, value_blocks))
    top_fin, total_fin, acc_fin = state_out
    attended = (acc_fin / total_fin[..., None]).astype(jnp.bfloat16)
    attended = (
        attended.reshape(kv_local, group_size, row_count, head_dim)
        .transpose(2, 0, 1, 3)
        .reshape(row_count, -1)
    )
    exchanged = lax.all_to_all(attended, "tp", split_axis=0, concat_axis=1, tiled=True)
    mixed_rows = jnp.dot(
        exchanged,
        lax.all_gather(out_weight, "tp", axis=0, tiled=True),
        preferred_element_type=jnp.float32,
    )
    return (latents.astype(jnp.float32) + gate_vec * normalize(mixed_rows)).astype(jnp.bfloat16)


def solution(mesh):
    torus = Mesh(mesh.devices.reshape(8, 4, mesh.shape["tp"]), ("sp_0", "sp_1", "tp"))
    placed = (
        P(SP_TP, None),
        P(SP, None),
        P(SP),
        P(SP),
        P(SP, "tp"),
        P(None, "tp"),
        P(None, "tp"),
        P(None, "tp"),
        P("tp", None),
        P(),
        P(),
    )
    return jax.shard_map(
        body, mesh=torus, in_specs=placed, out_specs=P(SP_TP, None), check_vma=False
    )
```

profile of v0, /device:TPU:1, one launch (start us, length us, event | category | flops | bytes accessed | tf_op | source)
XLA Modules:
  0.0 285.0 jit_solution(6609689054624795851)
XLA Ops:
  6.5 1.3 fusion.67
  7.8 17.5 %psum.14 = f32[2,768]{1,0:T(2,128)S(1)} all-reduce(f32[2,768]{1,0:T(2,128)S(1)} %fusion.67), channel_id=1, replica_groups=mesh['sp_0'=8,'sp_1'=4,'tp'=8] {'sp_0'}, use_global_device_ids=true, to_apply=%region_0.1 | all-reduce | flops 1536 | bytes 12288 | tf_op jit(solution)/shard_map/psum | solution.py:17
  25.3 8.6 %psum.15 = f32[2,768]{1,0:T(2,128)S(1)} all-reduce(f32[2,768]{1,0:T(2,128)S(1)} %psum.14), channel_id=1, replica_groups=mesh['sp_0'=8,'sp_1'=4,'tp'=8] {'sp_1'}, use_global_device_ids=true, to_apply=%region_1.2 | all-reduce | flops 1536 | bytes 12288 | tf_op jit(solution)/shard_map/psum | solution.py:17
  33.9 19.5 %all_gather.15 = f32[2,6144]{1,0:T(2,128)S(1)} all-gather(f32[2,768]{1,0:T(2,128)S(1)} %psum.15), channel_id=1, replica_groups=mesh['sp_0'=8,'sp_1'=4,'tp'=8] {'tp'}, dimensions={1}, use_global_device_ids=true | all-gather | bytes 55296 | tf_op jit(solution)/shard_map/all_gather | solution.py:88
  53.4 1.1 fusion.28
  54.5 1.8 fusion.31
  56.5 23.1 %all-gather.4.cloned.1.call-done = bf16[512,2048]{1,0:T(8,128)(2,1)} async-done(((bf16[64,2048]{1,0:T(8,128)(2,1)}), bf16[512,2048]{1,0:T(8,128)(2,1)}) %all-gather.4.cloned.1.call-update) | async-done | bytes 2097168 | tf_op jit(solution)/shard_map/all_gather | solution.py:94
  79.5 2.5 multiply_reduce_fusion.3
  82.7 2.5 fusion.22
  86.8 3.0 %multiply_cosine_fusion.1 = (f32[512,32]{1,0:T(8,128)S(1)}, f32[512,32]{1,0:T(8,128)}, f32[512,32]{1,0:T(8,128)}, f32[512,32]{1,0:T(8,128)}) fusion(f32[32]{0:T(128)S(1)} %multiply_power_fusion, f32[512]{0:T(512)S(1)} %get-tuple-element.112, f32[512]{0:T(512)S(1)} %get-tuple-element.113), kind=kLoop, calls=%fused_computation.50 | loop fusion | flops 32768 | bytes 266368 | tf_op jit(solution)/shard_map/cos | solution.py:40
  89.9 1.3 fusion.23
  91.2 1.4 multiply_reduce_fusion.4
  92.6 40.4 %all_gather.17 = bf16[512,2,128]{2,0,1:T(8,128)(2,1)} all-gather(bf16[16,2,128]{2,0,1:T(8,128)(2,1)S(1)} %pad_maximum_fusion.2), channel_id=1, replica_groups=mesh['sp_0'=8,'sp_1'=4,'tp'=8] {'sp_0','sp_1'}, dimensions={0}, use_global_device_ids=true | all-gather | bytes 270336 | tf_op jit(solution)/shard_map/all_gather | solution.py:23
  133.1 1.6 multiply_reduce_fusion.2
  134.7 1.3 copy.16
  136.2 1.6 fusion.33
  139.6 46.4 %all-gather.6.cloned.1.call-done = bf16[16384,2,128]{0,2,1:T(8,128)(2,1)} async-done(((bf16[512,2,128]{0,2,1:T(8,128)(2,1)}), bf16[16384,2,128]{0,2,1:T(8,128)(2,1)}) %all-gather.6.cloned.1.call-update) | async-done | bytes 8388624 | tf_op jit(solution)/shard_map/all_gather | solution.py:23
  186.1 5.8 %fusion.76 = (bf16[16384,1,128]{0,2,1:T(8,128)(2,1)}, bf16[16384,1,128]{0,2,1:T(8,128)(2,1)}) fusion(bf16[16384,2,128]{0,2,1:T(8,128)(2,1)} %all-gather.6.cloned.1.call-done), kind=kLoop, calls=%fused_computation.126 | loop fusion | bytes 16777216 | tf_op jit(solution)/shard_map/slice | solution.py:25
  191.9 6.3 %copy.23 = bf16[16384,1,128]{2,0,1:T(8,128)(2,1)} copy(bf16[16384,1,128]{0,2,1:T(8,128)(2,1)} %get-tuple-element.78) | data formatting | bytes 8388608 | tf_op jit(solution)/shard_map/while | solution.py:172
  198.2 6.5 %copy.24 = bf16[16384,1,128]{2,0,1:T(8,128)(2,1)} copy(bf16[16384,1,128]{0,2,1:T(8,128)(2,1)} %get-tuple-element.77) | data formatting | bytes 8388608 | tf_op jit(solution)/shard_map/while | solution.py:172
  204.7 52.6 %while.14 = (s32[]{:T(128)}, f32[1,1024]{1,0:T(1,128)S(1)}, f32[1,1024]{1,0:T(1,128)S(1)}, f32[1,1024,128]{2,1,0:T(8,128)S(1)}, bf16[8,2048,1,128]{3,1,2,0:T(8,1...) while((s32[]{:T(128)}, f32[1,1024]{1,0:T(1,128)S(1)}, ...), condition=%wide.region_12.13_spmd, body=%wide.region_9.12_spmd.sunk | while | flops 1090783232 | bytes 27590756 | solution.py:172
  204.7 2.3 multiply_reduce_fusion.6
  207.0 1.4 fusion.96
  208.5 2.8 fusion.97
  211.3 2.3 multiply_reduce_fusion.6
  213.6 1.4 fusion.96
  215.1 2.8 fusion.97
  217.9 2.3 multiply_reduce_fusion.6
  220.2 1.4 fusion.96
  221.6 2.8 fusion.97
  224.4 2.3 multiply_reduce_fusion.6
  226.8 1.4 fusion.96
  228.2 2.8 fusion.97
  231.0 2.3 multiply_reduce_fusion.6
  233.3 1.4 fusion.96
  234.8 2.8 fusion.97
  237.6 2.3 multiply_reduce_fusion.6
  239.9 1.4 fusion.96
  241.4 2.8 fusion.97
  244.2 2.3 multiply_reduce_fusion.6
  246.5 1.4 fusion.96
  247.9 2.8 fusion.97
  250.7 2.3 multiply_reduce_fusion.6
  253.0 1.4 fusion.96
  254.5 2.8 fusion.97
  258.0 14.5 %all_to_all.19 = bf16[8,64,256]{2,1,0:T(8,128)(2,1)S(1)} all-to-all(bf16[8,64,256]{2,1,0:T(8,128)(2,1)S(1)} %all_to_all.14), channel_id=1, replica_groups=mesh['sp_0'=8,'sp_1'=4,'tp'=8] {'tp'}, dimensions={0} | all-to-all | bytes 524288 | tf_op jit(solution)/shard_map/all_to_all | solution.py:180
  272.5 5.1 %multiply_reduce_fusion.1 = (f32[64]{0:T(128)S(1)}, f32[64,2048]{1,0:T(8,128)S(1)}) fusion(bf16[64,2048]{1,0:T(8,128)(2,1)S(1)} %bitcast.110, bf16[2048,2048]{1,0:T(8,128)(2,1)} %all-gather.8.cloned.1.call-done), kind=kOutput, calls=%fused_computation.39 | convolution fusion | flops 537132992 | bytes 9175296 | tf_op jit(solution)/shard_map/dot_general | solution.py:181
  277.6 0.9 fusion.32
  (69 shorter events, 5.5 us)
Async XLA Ops:
  6.5 126.6 %copy-start = (bf16[2048,256]{1,0:T(8,128)(2,1)S(1)}, bf16[2048,256]{1,0:T(8,128)(2,1)}, u32[]{:S(2)}) copy-start(bf16[2048,256]{1,0:T(8,128)(2,1)} %param.18) | copy-start | bytes 3145732
  6.5 75.5 %copy-start.5 = (f32[128]{0:T(128)S(1)}, f32[128]{0:T(128)}, u32[]{:S(2)}) copy-start(f32[128]{0:T(128)} %param.23) | copy-start | bytes 1540
  6.5 73.0 %all-gather.4.cloned.1.call-start = ((), (), s32[]{:S(2)}) async-start(), calls=%async_computation.1 | async-start | bytes 2359296 | tf_op jit(solution)/shard_map/all_gather | solution.py:94
  56.4 129.7 %all-gather.6.cloned.1.call-start = ((), (), s32[]{:S(2)}) async-start(), calls=%async_computation.2 | async-start | bytes 8650752 | tf_op jit(solution)/shard_map/all_gather | solution.py:23
  56.4 33.3 %copy-start.4 = (bf16[16,2048]{1,0:T(8,128)(2,1)S(1)}, bf16[16,2048]{1,0:T(8,128)(2,1)}, u32[]{:S(2)}) copy-start(bf16[16,2048]{1,0:T(8,128)(2,1)} %param.14) | copy-start | bytes 196612
  82.1 51.0 %copy-start.1 = (bf16[512,2048]{1,0:T(8,128)(2,1)S(1)}, bf16[512,2048]{1,0:T(8,128)(2,1)}, u32[]{:S(2)}) copy-start(bf16[512,2048]{1,0:T(8,128)(2,1)} %all-gather.4.cloned.1.call-done) | copy-start | bytes 6291460
  86.0 49.9 %copy-start.6 = (f32[128]{0:T(128)S(1)}, f32[128]{0:T(128)}, u32[]{:S(2)}) copy-start(f32[128]{0:T(128)} %param.22) | copy-start | bytes 1540
  86.0 186.5 %all-gather.8.cloned.1.call-start = ((), (), s32[]{:S(2)}) async-start(), calls=%async_computation.3 | async-start | bytes 9437184 | tf_op jit(solution)/shard_map/all_gather | solution.py:183
  134.7 3.5 %copy-start.3 = (bf16[512,2,128]{2,0,1:T(8,128)(2,1)S(1)}, bf16[512,2,128]{2,0,1:T(8,128)(2,1)}, u32[]{:S(2)}) copy-start(bf16[512,2,128]{2,0,1:T(8,128)(2,1)} %all_gather.17) | copy-start | bytes 786436
  272.5 5.1 %copy-start.2 = (bf16[64,2048]{1,0:T(8,128)(2,1)S(1)}, bf16[64,2048]{1,0:T(8,128)(2,1)}, u32[]{:S(2)}) copy-start(bf16[64,2048]{1,0:T(8,128)(2,1)} %param.13) | copy-start | bytes 786436
Sparse Core Ops, SparseCore 0:
  56.5 23.0 all-gather.3
  86.1 99.8 all-gather.5
  187.9 54.6 all-gather.7
where the time goes:
time: 286 us; the launch traced here: 285 us
  blocking collectives  100 us (35%)
  waiting for transfers between devices  70.3 us (25%)
  matrix products  57.2 us (20%)
  other arithmetic  22.9 us (8%)
  local copies, waits for them, and re-layouts  20.4 us (7%)
  between operations  13.4 us (5%)
    all_gather x1, waiting for transfers between devices, side_by_side(): filled, at, done = (lax.all_gather(both, axis, axis=dim, tiled=True), 0, [])  46.4 us
    all_gather x1, blocking collectives, side_by_side(): filled, at, done = (lax.all_gather(both, axis, axis=dim, tiled=True), 0, [])  40.4 us
    psum x2, blocking collectives, over_axes(): value = lax.psum(value, axis)  26.1 us
    all_gather x1, waiting for transfers between devices, body(): piece = lax.all_gather(normalised_rows, 'tp', axis=0, tiled=True)  23.1 us
    dot_general x8, matrix products, update(): jnp.einsum('hqk,khd->hqd', weights_now.astype(jnp.bfloat16), value_block,...  22.2 us
    all_gather x1, blocking collectives, body(): modulation = lax.all_gather(summed, 'tp', axis=1, tiled=True)  19.5 us
    dot_general x8, matrix products, update(): jnp.einsum('hqd,khd->hqk', grouped, key_block, preferred_element_type=jnp...  18.4 us
    all_to_all x1, blocking collectives, body(): lax.all_to_all(attended, 'tp', split_axis=0, concat_axis=1, tiled=True)  14.5 us
  transfers between devices with their start and end apart: 3, of which 2 were waited for; matrix products, arithmetic and copies ran while one was open for 29% of the time, Pallas kernels for 0%

commit v1 on v0

--- a/solution.py
+++ b/solution.py
@@ -10,6 +10,15 @@
 SP_TP = ("sp_0", "sp_1", "tp")
 NORM_EPS = 1e-06
 ROPE_BASE = 10000.0
+
+
+def post_columns_all(target):
+    return jnp.concatenate(
+        jax.lax.all_to_all(
+            jnp.stack(jnp.split(target, jax.lax.axis_size("tp"), axis=0), axis=0), "tp", 0, 0
+        ),
+        axis=1,
+    )
 
 
 def over_axes(value, axes):
@@ -177,7 +186,7 @@
         .transpose(2, 0, 1, 3)
         .reshape(row_count, -1)
     )
-    exchanged = lax.all_to_all(attended, "tp", split_axis=0, concat_axis=1, tiled=True)
+    exchanged = post_columns_all(attended)
     mixed_rows = jnp.dot(
         exchanged,
         lax.all_gather(out_weight, "tp", axis=0, tiled=True),

time: 286 us -> 287 us (level)
  transfers between devices with their start and end apart: 3 -> 3, of which waited for: 2 -> 2; matrix products, arithmetic and copies ran while one was open for 29% -> 30% of each run, Pallas kernels for 0% -> 0%
where the time goes in v1:
time: 287 us; the launch traced here: 285 us
  blocking collectives  100 us (35%)
  waiting for transfers between devices  70.2 us (24%)
  matrix products  57.2 us (20%)
  other arithmetic  22.9 us (8%)
  local copies, waits for them, and re-layouts  20.7 us (7%)
  between operations  13.5 us (5%)
    all_gather x1, waiting for transfers between devices, side_by_side(): filled, at, done = (lax.all_gather(both, axis, axis=dim, tiled=True), 0, [])  46.4 us
    all_gather x1, blocking collectives, side_by_side(): filled, at, done = (lax.all_gather(both, axis, axis=dim, tiled=True), 0, [])  40.4 us
    psum x2, blocking collectives, over_axes(): value = lax.psum(value, axis)  26.1 us
    all_gather x1, waiting for transfers between devices, body(): piece = lax.all_gather(normalised_rows, 'tp', axis=0, tiled=True)  23.1 us
    dot_general x8, matrix products, update(): jnp.einsum('hqk,khd->hqd', weights_now.astype(jnp.bfloat16), value_block,...  22.2 us
    all_gather x1, blocking collectives, body(): modulation = lax.all_gather(summed, 'tp', axis=1, tiled=True)  19.5 us
    dot_general x8, matrix products, update(): jnp.einsum('hqd,khd->hqk', grouped, key_block, preferred_element_type=jnp...  18.4 us
    all_to_all x1, blocking collectives, post_columns_all(): jax.lax.all_to_all(jnp.stack(jnp.split(target, jax.lax.axis_size('tp'), a...  14.5 us
  transfers between devices with their start and end apart: 3, of which 2 were waited for; matrix products, arithmetic and copies ran while one was open for 30% of the time, Pallas kernels for 0%

profile of v1, /device:TPU:1, one launch (start us, length us, event | category | flops | bytes accessed | tf_op | source)
XLA Modules:
  0.0 285.4 jit_solution(9054854437950963230)
XLA Ops:
  6.5 1.3 fusion.67
  7.8 17.5 %psum.14 = f32[2,768]{1,0:T(2,128)S(1)} all-reduce(f32[2,768]{1,0:T(2,128)S(1)} %fusion.67), channel_id=1, replica_groups=mesh['sp_0'=8,'sp_1'=4,'tp'=8] {'sp_0'}, use_global_device_ids=true, to_apply=%region_0.1 | all-reduce | flops 1536 | bytes 12288 | tf_op jit(solution)/shard_map/psum | solution.py:26
  25.3 8.6 %psum.15 = f32[2,768]{1,0:T(2,128)S(1)} all-reduce(f32[2,768]{1,0:T(2,128)S(1)} %psum.14), channel_id=1, replica_groups=mesh['sp_0'=8,'sp_1'=4,'tp'=8] {'sp_1'}, use_global_device_ids=true, to_apply=%region_1.2 | all-reduce | flops 1536 | bytes 12288 | tf_op jit(solution)/shard_map/psum | solution.py:26
  33.9 19.5 %all_gather.15 = f32[2,6144]{1,0:T(2,128)S(1)} all-gather(f32[2,768]{1,0:T(2,128)S(1)} %psum.15), channel_id=1, replica_groups=mesh['sp_0'=8,'sp_1'=4,'tp'=8] {'tp'}, dimensions={1}, use_global_device_ids=true | all-gather | bytes 55296 | tf_op jit(solution)/shard_map/all_gather | solution.py:97
  53.4 1.1 fusion.28
  54.5 1.8 fusion.31
  56.5 23.1 %all-gather.4.cloned.1.call-done = bf16[512,2048]{1,0:T(8,128)(2,1)} async-done(((bf16[64,2048]{1,0:T(8,128)(2,1)}), bf16[512,2048]{1,0:T(8,128)(2,1)}) %all-gather.4.cloned.1.call-update) | async-done | bytes 2097168 | tf_op jit(solution)/shard_map/all_gather | solution.py:103
  79.5 2.5 multiply_reduce_fusion.3
  82.7 2.5 fusion.22
  86.8 3.0 %multiply_cosine_fusion.1 = (f32[512,32]{1,0:T(8,128)S(1)}, f32[512,32]{1,0:T(8,128)}, f32[512,32]{1,0:T(8,128)}, f32[512,32]{1,0:T(8,128)}) fusion(f32[32]{0:T(128)S(1)} %multiply_power_fusion, f32[512]{0:T(512)S(1)} %get-tuple-element.120, f32[512]{0:T(512)S(1)} %get-tuple-element.121), kind=kLoop, calls=%fused_computation.50 | loop fusion | flops 32768 | bytes 266368 | tf_op jit(solution)/shard_map/cos | solution.py:49
  89.9 1.4 multiply_reduce_fusion.4
  91.3 1.3 fusion.23
  92.6 40.4 %all_gather.17 = bf16[512,2,128]{2,0,1:T(8,128)(2,1)} all-gather(bf16[16,2,128]{2,0,1:T(8,128)(2,1)S(1)} %pad_maximum_fusion.2), channel_id=1, replica_groups=mesh['sp_0'=8,'sp_1'=4,'tp'=8] {'sp_0','sp_1'}, dimensions={0}, use_global_device_ids=true | all-gather | bytes 270336 | tf_op jit(solution)/shard_map/all_gather | solution.py:32
  133.1 1.6 multiply_reduce_fusion.2
  134.7 1.3 copy.16
  136.2 1.6 fusion.33
  139.6 46.4 %all-gather.6.cloned.1.call-done = bf16[16384,2,128]{0,2,1:T(8,128)(2,1)} async-done(((bf16[512,2,128]{0,2,1:T(8,128)(2,1)}), bf16[16384,2,128]{0,2,1:T(8,128)(2,1)}) %all-gather.6.cloned.1.call-update) | async-done | bytes 8388624 | tf_op jit(solution)/shard_map/all_gather | solution.py:32
  186.1 5.8 %fusion.76 = (bf16[16384,1,128]{0,2,1:T(8,128)(2,1)}, bf16[16384,1,128]{0,2,1:T(8,128)(2,1)}) fusion(bf16[16384,2,128]{0,2,1:T(8,128)(2,1)} %all-gather.6.cloned.1.call-done), kind=kLoop, calls=%fused_computation.134 | loop fusion | bytes 16777216 | tf_op jit(solution)/shard_map/slice | solution.py:34
  191.9 6.3 %copy.23 = bf16[16384,1,128]{2,0,1:T(8,128)(2,1)} copy(bf16[16384,1,128]{0,2,1:T(8,128)(2,1)} %get-tuple-element.78) | data formatting | bytes 8388608 | tf_op jit(solution)/shard_map/while | solution.py:181
  198.2 6.5 %copy.24 = bf16[16384,1,128]{2,0,1:T(8,128)(2,1)} copy(bf16[16384,1,128]{0,2,1:T(8,128)(2,1)} %get-tuple-element.77) | data formatting | bytes 8388608 | tf_op jit(solution)/shard_map/while | solution.py:181
  204.7 52.6 %while.14 = (s32[]{:T(128)}, f32[1,1024]{1,0:T(1,128)S(1)}, f32[1,1024]{1,0:T(1,128)S(1)}, f32[1,1024,128]{2,1,0:T(8,128)S(1)}, bf16[8,2048,1,128]{3,1,2,0:T(8,1...) while((s32[]{:T(128)}, f32[1,1024]{1,0:T(1,128)S(1)}, ...), condition=%wide.region_12.13_spmd, body=%wide.region_9.12_spmd.sunk | while | flops 1090783232 | bytes 27591764 | solution.py:181
  204.7 2.3 multiply_reduce_fusion.6
  207.0 1.4 fusion.97
  208.5 2.8 fusion.98
  211.3 2.3 multiply_reduce_fusion.6
  213.6 1.4 fusion.97
  215.1 2.8 fusion.98
  217.9 2.3 multiply_reduce_fusion.6
  220.2 1.4 fusion.97
  221.6 2.8 fusion.98
  224.4 2.3 multiply_reduce_fusion.6
  226.8 1.4 fusion.97
  228.2 2.8 fusion.98
  231.0 2.3 multiply_reduce_fusion.6
  233.3 1.4 fusion.97
  234.8 2.8 fusion.98
  237.6 2.3 multiply_reduce_fusion.6
  239.9 1.4 fusion.97
  241.4 2.8 fusion.98
  244.2 2.3 multiply_reduce_fusion.6
  246.5 1.4 fusion.97
  247.9 2.8 fusion.98
  250.7 2.3 multiply_reduce_fusion.6
  253.0 1.4 fusion.97
  254.5 2.8 fusion.98
  258.3 14.5 %all_to_all.5 = bf16[8,64,256]{2,1,0:T(8,128)(2,1)S(1)} all-to-all(bf16[8,64,256]{2,1,0:T(8,128)(2,1)S(1)} %constant_dynamic-update-slice_fusion), channel_id=1, replica_groups=mesh['sp_0'=8,'sp_1'=4,'tp'=8] {'tp'}, dimensions={0} | all-to-all | bytes 524288 | tf_op jit(solution)/shard_map/all_to_all | solution.py:17
  272.9 5.1 %multiply_reduce_fusion.1 = (f32[64]{0:T(128)S(1)}, f32[64,2048]{1,0:T(8,128)S(1)}) fusion(bf16[64,2048]{1,0:T(8,128)(2,1)S(1)} %bitcast.124, bf16[2048,2048]{1,0:T(8,128)(2,1)} %all-gather.8.cloned.1.call-done), kind=kOutput, calls=%fused_computation.39 | convolution fusion | flops 537132992 | bytes 9175296 | tf_op jit(solution)/shard_map/dot_general | solution.py:190
  278.0 0.9 fusion.32
  (85 shorter events, 5.8 us)
Async XLA Ops:
  6.5 126.6 %copy-start = (bf16[2048,256]{1,0:T(8,128)(2,1)S(1)}, bf16[2048,256]{1,0:T(8,128)(2,1)}, u32[]{:S(2)}) copy-start(bf16[2048,256]{1,0:T(8,128)(2,1)} %param.18) | copy-start | bytes 3145732
  6.5 75.5 %copy-start.5 = (f32[128]{0:T(128)S(1)}, f32[128]{0:T(128)}, u32[]{:S(2)}) copy-start(f32[128]{0:T(128)} %param.23) | copy-start | bytes 1540
  6.5 73.0 %all-gather.4.cloned.1.call-start = ((), (), s32[]{:S(2)}) async-start(), calls=%async_computation.1 | async-start | bytes 2359296 | tf_op jit(solution)/shard_map/all_gather | solution.py:103
  56.4 129.7 %all-gather.6.cloned.1.call-start = ((), (), s32[]{:S(2)}) async-start(), calls=%async_computation.2 | async-start | bytes 8650752 | tf_op jit(solution)/shard_map/all_gather | solution.py:32
  56.4 33.3 %copy-start.4 = (bf16[16,2048]{1,0:T(8,128)(2,1)S(1)}, bf16[16,2048]{1,0:T(8,128)(2,1)}, u32[]{:S(2)}) copy-start(bf16[16,2048]{1,0:T(8,128)(2,1)} %param.14) | copy-start | bytes 196612
  82.1 51.0 %copy-start.1 = (bf16[512,2048]{1,0:T(8,128)(2,1)S(1)}, bf16[512,2048]{1,0:T(8,128)(2,1)}, u32[]{:S(2)}) copy-start(bf16[512,2048]{1,0:T(8,128)(2,1)} %all-gather.4.cloned.1.call-done) | copy-start | bytes 6291460
  86.0 49.9 %copy-start.6 = (f32[128]{0:T(128)S(1)}, f32[128]{0:T(128)}, u32[]{:S(2)}) copy-start(f32[128]{0:T(128)} %param.22) | copy-start | bytes 1540
  86.0 186.8 %all-gather.8.cloned.1.call-start = ((), (), s32[]{:S(2)}) async-start(), calls=%async_computation.3 | async-start | bytes 9437184 | tf_op jit(solution)/shard_map/all_gather | solution.py:192
  134.7 3.5 %copy-start.3 = (bf16[512,2,128]{2,0,1:T(8,128)(2,1)S(1)}, bf16[512,2,128]{2,0,1:T(8,128)(2,1)}, u32[]{:S(2)}) copy-start(bf16[512,2,128]{2,0,1:T(8,128)(2,1)} %all_gather.17) | copy-start | bytes 786436
  272.9 5.1 %copy-start.2 = (bf16[64,2048]{1,0:T(8,128)(2,1)S(1)}, bf16[64,2048]{1,0:T(8,128)(2,1)}, u32[]{:S(2)}) copy-start(bf16[64,2048]{1,0:T(8,128)(2,1)} %param.13) | copy-start | bytes 786436
Sparse Core Ops, SparseCore 0:
  56.5 23.0 all-gather.3
  86.1 99.8 all-gather.5
  187.9 54.6 all-gather.7
